TPU v7x, 32 devices: a whole 2x2x4 slice. The times are simulated.
32 devices in a mesh: rep: 2 (over y), fs: 4 (over z), tp: 4 (over x, core).
Axes of the slice: x: 2, y: 2, z: 4, core: 2. Of those that a mesh axis runs over, the one named last changes fastest.
Arguments:
- stream: bfloat16 [4096, 2048], P(('rep', 'fs'), 'tp'), parts along dimension 0, may hold values from -6 to 6
- in_weight: bfloat16 [2048, 1024], P('fs', 'tp'), may hold values from -0.125 to 0.125
- pool_weight: bfloat16 [8, 128, 128], P('tp'), may hold values from -0.5 to 0.5
- pool_scale: bfloat16 [1024], P('tp'), may hold values from 0.099609375 to 1.8984375
- out_weight: bfloat16 [1024, 2048], P('tp', 'fs'), may hold values from -0.1875 to 0.1875
- mix_gain: bfloat16 [2048], replicated, may hold values from 0.099609375 to 1.8984375
- ffn_gain: bfloat16 [2048], replicated, may hold values from 0.099609375 to 1.8984375
- gate_weight: bfloat16 [2048, 5632], P('fs', 'tp'), may hold values from -0.125 to 0.125
- up_weight: bfloat16 [2048, 5632], P('fs', 'tp'), may hold values from -0.125 to 0.125
- down_weight: bfloat16 [5632, 2048], P('tp', 'fs'), may hold values from -0.078125 to 0.078125
Outputs:
- result: bfloat16 [4096, 2048], P(('rep', 'fs'), 'tp'), parts along dimension 0
There are 2 independent parts, one for each index of `rep`. A program takes and returns all parts, laid end to end along the dimension named above; an argument that names none is the same for every part. Nothing has to cross between parts.
All inputs are finite; a program needn't handle non-finite values.
Results may differ from a plain program's by a relative error of at most 0.015.
Values may be sent and summed in bfloat16 or wider, within the bound.
A program may use at most 64 MiB of HBM per device.

v0:
```python
import jax
import jax.numpy as jnp
from jax import lax
from jax.sharding import PartitionSpec as P

GROUPS = 8
SEQ = 128


epsilon = 1e-06


def root_norm(values, gain_vec):
    widened = values.astype(jnp.float32)
    scaled = widened * lax.rsqrt(jnp.mean(widened * widened, axis=-1, keepdims=True) + epsilon)
    return (scaled * gain_vec.astype(jnp.float32)).astype(jnp.bfloat16)


def window_tables(first_group, group_count, seq_len, total_groups):
    group_ids = first_group + jnp.arange(group_count, dtype=jnp.int32)
    reaches = jnp.left_shift(jnp.int32(2), 4 * group_ids // total_groups)
    query_pos = jnp.arange(seq_len, dtype=jnp.int32)[:, None]
    earlier = jnp.arange(seq_len, dtype=jnp.int32)[None, :]
    inside = (earlier <= query_pos)[None] & (
        earlier[None] > query_pos[None] - reaches[:, None, None]
    )
    counts = jnp.minimum(query_pos[:, 0][None, :] + 1, reaches[:, None]).astype(jnp.float32)
    return (inside, counts)


def full_rows(values):
    return lax.all_gather(values, "tp", axis=1, tiled=True)


def on_device(
    stream,
    in_weight,
    pool_weight,
    pool_scale,
    out_weight,
    mix_gain,
    ffn_gain,
    gate_weight,
    up_weight,
    down_weight,
):
    normed = root_norm(full_rows(stream), mix_gain)
    tokens = normed.shape[0]
    local_groups = pool_weight.shape[0]
    group_dim = pool_weight.shape[1]
    pooled_in = jnp.dot(
        normed,
        lax.all_gather(in_weight, "fs", axis=0, tiled=True),
        preferred_element_type=jnp.float32,
    ).astype(jnp.bfloat16)
    first_group = lax.axis_index("tp") * local_groups
    inside, counts = window_tables(first_group, local_groups, SEQ, GROUPS)
    grouped = pooled_in.reshape(tokens // SEQ, SEQ, local_groups, group_dim)
    window_sums = jnp.einsum(
        "gts,nsgc->ntgc", inside.astype(jnp.bfloat16), grouped, preferred_element_type=jnp.float32
    )
    contrast = (window_sums / counts.T[None, :, :, None] - grouped.astype(jnp.float32)).astype(
        jnp.bfloat16
    )
    mixed_out = jnp.einsum(
        "ntgc,gcd->ntgd", contrast, pool_weight, preferred_element_type=jnp.float32
    )
    group_out = (
        mixed_out.reshape(tokens, local_groups * group_dim) * pool_scale.astype(jnp.float32)
    ).astype(jnp.bfloat16)
    collected = lax.all_gather(out_weight, "fs", axis=1, tiled=True)
    tp_count = lax.axis_size("tp")
    own_width = stream.shape[1]
    block_cols = lax.all_to_all(collected, "tp", split_axis=1, concat_axis=0, tiled=True)
    all_channels = lax.all_gather(group_out, "tp", axis=1, tiled=True)
    block_width = group_out.shape[1]
    products = jnp.einsum(
        "tkc,kcd->ktd",
        all_channels.reshape(tokens, tp_count, block_width),
        block_cols.reshape(tp_count, block_width, own_width),
        preferred_element_type=jnp.float32,
    )
    rounded = lax.optimization_barrier(products.astype(jnp.bfloat16))
    mixer_sum = jnp.sum(rounded.astype(jnp.float32), axis=0)
    middle = (stream.astype(jnp.float32) + mixer_sum).astype(jnp.bfloat16)
    normed_ffn = root_norm(full_rows(middle), ffn_gain)
    gate_cols, up_cols, down_rows = (
        lax.all_gather(gate_weight, "fs", axis=0, tiled=True),
        lax.all_gather(up_weight, "fs", axis=0, tiled=True),
        lax.all_gather(down_weight, "fs", axis=1, tiled=True),
    )
    gate_acts = jnp.dot(normed_ffn, gate_cols, preferred_element_type=jnp.float32)
    up_acts = jnp.dot(normed_ffn, up_cols, preferred_element_type=jnp.float32)
    hidden = (jax.nn.silu(gate_acts) * up_acts).astype(jnp.bfloat16)
    ffn_partials = jnp.dot(hidden, down_rows, preferred_element_type=jnp.float32)
    ffn_sum = lax.psum_scatter(
        ffn_partials.astype(jnp.bfloat16), "tp", scatter_dimension=1, tiled=True
    ).astype(jnp.float32)
    return (middle.astype(jnp.float32) + ffn_sum).astype(jnp.bfloat16)


def solution(mesh):
    return jax.shard_map(
        on_device,
        mesh=mesh,
        in_specs=(
            P(("rep", "fs"), "tp"),
            P("fs", "tp"),
            P("tp", None, None),
            P("tp"),
            P("tp", "fs"),
            P(),
            P(),
            P("fs", "tp"),
            P("fs", "tp"),
            P("tp", "fs"),
        ),
        out_specs=P(("rep", "fs"), "tp"),
        check_vma=False,
    )
```

profile of v0, /device:TPU:0, one launch (start us, length us, event | category | flops | bytes accessed | tf_op | source)
XLA Modules:
  0.0 515.2 jit_solution(7904418441016153907)
XLA Ops:
  6.5 0.7 all-gather.9.cloned.1.call-update
  7.3 0.7 all-gather.11.cloned.1.call-update
  8.1 1.8 copy.15
  10.1 0.7 convert_element_type.71
  10.8 0.7 convert_element_type.77
  11.5 22.7 %all-gather.9.cloned.1.call-done = bf16[512,2048]{1,0:T(8,128)(2,1)} async-done(((bf16[512,512]{1,0:T(8,128)(2,1)}), bf16[512,2048]{1,0:T(8,128)(2,1)}) %all-gather.9.cloned.1.call-update) | async-done | bytes 2097168 | tf_op jit(solution)/shard_map/all_gather | solution.py:32
  34.2 2.1 fusion
  36.3 27.5 %all-gather.11.cloned.1.call-done = bf16[2048,256]{1,0:T(8,128)(2,1)} async-done(((bf16[512,256]{1,0:T(8,128)(2,1)}), bf16[2048,256]{1,0:T(8,128)(2,1)}) %all-gather.11.cloned.1.call-update) | async-done | bytes 1048592 | tf_op jit(solution)/shard_map/all_gather | solution.py:53
  63.8 2.6 fusion.14
  66.5 0.5 convolution_bitcast_fusion
  67.0 0.4 copy.13
  67.4 0.7 fusion.22
  68.1 24.6 %all-gather.15.cloned.1.call-done = bf16[256,2048]{0,1:T(8,128)(2,1)} async-done(((bf16[256,512]{0,1:T(8,128)(2,1)}), bf16[256,2048]{0,1:T(8,128)(2,1)}) %all-gather.15.cloned.1.call-update) | async-done | bytes 1048592 | tf_op jit(solution)/shard_map/all_gather | solution.py:71
  92.8 2.3 copy.16
  95.1 3.5 all-to-all-start
  98.6 17.5 %all-gather.13.cloned.1.call-done = bf16[512,1024]{1,0:T(8,128)(2,1)} async-done(((bf16[512,256]{1,0:T(8,128)(2,1)}), bf16[512,1024]{1,0:T(8,128)(2,1)}) %all-gather.13.cloned.1.call-update) | async-done | bytes 1048592 | tf_op jit(solution)/shard_map/all_gather | solution.py:75
  116.1 1.5 copy.14
  117.6 1.0 all-to-all-done
  118.6 0.8 convolution_convert_fusion.1
  119.7 1.0 add_convert_fusion.1
  120.7 0.5 all-gather.19.cloned.1.call-update
  121.3 0.7 all-gather.21.cloned.1.call-update
  122.0 0.7 all-gather.23.cloned.1.call-update
  123.0 19.4 %all-gather.17.cloned.1.call-done = bf16[512,2048]{1,0:T(8,128)(2,1)} async-done(((bf16[512,512]{1,0:T(8,128)(2,1)}), bf16[512,2048]{1,0:T(8,128)(2,1)}) %all-gather.17.cloned.1.call-update) | async-done | bytes 2097168 | tf_op jit(solution)/shard_map/all_gather | solution.py:32
  142.4 2.1 fusion.3
  144.5 106.1 %all-gather.19.cloned.1.call-done = bf16[2048,1408]{1,0:T(8,128)(2,1)} async-done(((bf16[512,1408]{1,0:T(8,128)(2,1)}), bf16[2048,1408]{1,0:T(8,128)(2,1)}) %all-gather.19.cloned.1.call-update) | async-done | bytes 5767184 | tf_op jit(solution)/shard_map/all_gather | solution.py:88
  250.6 8.3 %fusion.20 = f32[512,1408]{1,0:T(8,128)} fusion(bf16[2048,1408]{1,0:T(8,128)(2,1)} %all-gather.19.cloned.1.call-done, bf16[512,2048]{1,0:T(8,128)(2,1)} %all-gather.17.cloned.1.call-done, f32[2048]{0:T(1024)S(1)} %convert_element_type.84, f32[512]{0:T(512)S(1)} %add_rsqrt_fusion), kind=kOutput, calls=%fused_computation.27 | convolution fusion | flops 2956984320 | bytes 10758144 | tf_op jit(solution)/shard_map/dot_general | solution.py:92
  258.9 98.3 %all-gather.21.cloned.1.call-done = bf16[2048,1408]{1,0:T(8,128)(2,1)} async-done(((bf16[512,1408]{1,0:T(8,128)(2,1)}), bf16[2048,1408]{1,0:T(8,128)(2,1)}) %all-gather.21.cloned.1.call-update) | async-done | bytes 5767184 | tf_op jit(solution)/shard_map/all_gather | solution.py:89
  357.1 106.5 %all-gather.23.cloned.1.call-done = bf16[1408,2048]{1,0:T(8,128)(2,1)} async-done(((bf16[1408,512]{1,0:T(8,128)(2,1)}), bf16[1408,2048]{1,0:T(8,128)(2,1)}) %all-gather.23.cloned.1.call-update) | async-done | bytes 5767184 | tf_op jit(solution)/shard_map/all_gather | solution.py:90
  463.7 13.4 %convolution_convert_fusion = bf16[512,2048]{1,0:T(8,128)(2,1)} fusion(bf16[1408,2048]{1,0:T(8,128)(2,1)} %all-gather.23.cloned.1.call-done, bf16[2048,1408]{1,0:T(8,128)(2,1)} %all-gather.21.cloned.1.call-done, f32[512,1408]{1,0:T(8,128)} %fusion.20, bf16[512,2048]{1,0:T(8,128)(2,1)S(1)} %copy-done.2, f32[2048]{0:T(1024)S(1)} %convert_element_type.84, ...), kind=kOutput, calls=%fused_computation.13 | convolution fusion | flops 5915148288 | bytes 18622464 | tf_op jit(solution)/shard_map/dot_general | solution.py:95
  477.1 29.6 %reduce-scatter.2.cloned.1.call-done = bf16[512,512]{1,0:T(8,128)(2,1)} async-done(((bf16[512,2048]{1,0:T(8,128)(2,1)}), bf16[512,512]{1,0:T(8,128)(2,1)}) %reduce-scatter.2.cloned.1.call-update) | async-done | bytes 524304 | tf_op jit(solution)/shard_map/reduce_scatter | solution.py:96
  506.7 2.0 add_convert_fusion
  (33 shorter events, 1.2 us)
Async XLA Ops:
  6.5 60.0 %copy-start = (bf16[2,128,128]{2,1,0:T(8,128)(2,1)S(1)}, bf16[2,128,128]{2,1,0:T(8,128)(2,1)}, u32[]{:S(2)}) copy-start(bf16[2,128,128]{2,1,0:T(8,128)(2,1)} %param.12) | copy-start | bytes 196612
  6.5 27.7 %all-gather.9.cloned.1.call-start = ((), (), s32[]{:S(2)}) async-start(), calls=%async_computation.2 | async-start | bytes 2621440 | tf_op jit(solution)/shard_map/all_gather | solution.py:32
  7.3 56.5 %all-gather.11.cloned.1.call-start = ((), (), s32[]{:S(2)}) async-start(), calls=%async_computation.3 | async-start | bytes 1310720 | tf_op jit(solution)/shard_map/all_gather | solution.py:53
  8.0 84.8 %all-gather.15.cloned.1.call-start = ((), (), s32[]{:S(2)}) async-start(), calls=%async_computation.5 | async-start | bytes 1310720 | tf_op jit(solution)/shard_map/all_gather | solution.py:71
  9.9 106.2 %all-gather.13.cloned.1.call-start = ((), (), s32[]{:S(2)}) async-start(), calls=%async_computation.4 | async-start | bytes 1310720 | tf_op jit(solution)/shard_map/all_gather | solution.py:75
  95.1 23.5 %all-to-all-start = ((bf16[256,4,512]{2,0,1:T(8,128)(2,1)}), bf16[256,4,512]{2,0,1:T(8,128)(2,1)S(1)}, u32[]{:S(2)}, u32[]{:S(2)}) async-start(bf16[256,4,512]{2,0,1:T(8,128)(2,1)} %copy.16), calls=%async_computation | async-start | bytes 2097152 | tf_op jit(solution)/shard_map/all_to_all | solution.py:74
  98.6 43.8 %all-gather.17.cloned.1.call-start = ((), (), s32[]{:S(2)}) async-start(), calls=%async_computation.6 | async-start | bytes 2621440 | tf_op jit(solution)/shard_map/all_gather | solution.py:32
  118.6 1.1 copy-start.3
  120.6 2.3 copy-start.4
  120.7 129.9 %all-gather.19.cloned.1.call-start = ((), (), s32[]{:S(2)}) async-start(), calls=%async_computation.7 | async-start | bytes 7208960 | tf_op jit(solution)/shard_map/all_gather | solution.py:88
  121.3 235.9 %all-gather.21.cloned.1.call-start = ((), (), s32[]{:S(2)}) async-start(), calls=%async_computation.8 | async-start | bytes 7208960 | tf_op jit(solution)/shard_map/all_gather | solution.py:89
  122.0 341.7 %all-gather.23.cloned.1.call-start = ((), (), s32[]{:S(2)}) async-start(), calls=%async_computation.9 | async-start | bytes 7208960 | tf_op jit(solution)/shard_map/all_gather | solution.py:90
  122.8 383.9 %reduce-scatter.2.cloned.1.call-start = ((), (), s32[]{:S(2)}) async-start(), calls=%async_computation.10 | async-start | bytes 2621440 | tf_op jit(solution)/shard_map/reduce_scatter | solution.py:96
  144.5 319.2 %copy-start.2 = (bf16[512,2048]{1,0:T(8,128)(2,1)S(1)}, bf16[512,2048]{1,0:T(8,128)(2,1)}, u32[]{:S(2)}) copy-start(bf16[512,2048]{1,0:T(8,128)(2,1)} %all-gather.17.cloned.1.call-done) | copy-start | bytes 6291460
  258.9 247.8 %copy-start.1 = (bf16[512,512]{1,0:T(8,128)(2,1)S(1)}, bf16[512,512]{1,0:T(8,128)(2,1)}, u32[]{:S(2)}) copy-start(bf16[512,512]{1,0:T(8,128)(2,1)} %add_convert_fusion.1) | copy-start | bytes 1572868
Sparse Core Ops, SparseCore 0:
  8.9 25.2 all-gather.8
  35.8 27.9 all-gather.10
  65.4 27.3 all-gather.14
  94.2 21.8 all-gather.12
  120.8 21.5 all-gather.16
  143.9 106.6 all-gather.18
  252.1 104.9 all-gather.20
  358.7 104.9 all-gather.22
  477.2 29.4 reduce-scatter.1
where the time goes:
time: 516 us; the launch traced here: 515 us
  waiting for transfers between devices  457 us (89%)
  matrix products  25.5 us (5%)
  between operations  13.3 us (3%)
  other arithmetic  9.67 us (2%)
  local copies, waits for them, and re-layouts  6.08 us (1%)
    all_gather x1, waiting for transfers between devices, on_device(): lax.all_gather(down_weight, 'fs', axis=1, tiled=True)  107 us
    all_gather x1, waiting for transfers between devices, on_device(): lax.all_gather(gate_weight, 'fs', axis=0, tiled=True)  106 us
    all_gather x1, waiting for transfers between devices, on_device(): lax.all_gather(up_weight, 'fs', axis=0, tiled=True)  98.3 us
    all_gather x2, waiting for transfers between devices, full_rows(): return lax.all_gather(values, 'tp', axis=1, tiled=True)  42.2 us
    reduce_scatter x1, waiting for transfers between devices, on_device(): lax.psum_scatter(ffn_partials.astype(jnp.bfloat16), 'tp', scatter_dimensi...  29.6 us
    all_gather x1, waiting for transfers between devices, on_device(): lax.all_gather(in_weight, 'fs', axis=0, tiled=True)  27.5 us
    all_gather x1, waiting for transfers between devices, on_device(): collected = lax.all_gather(out_weight, 'fs', axis=1, tiled=True)  24.6 us
    all_gather x1, waiting for transfers between devices, on_device(): all_channels = lax.all_gather(group_out, 'tp', axis=1, tiled=True)  17.5 us
  transfers between devices with their start and end apart: 10, of which 10 were waited for; matrix products, arithmetic and copies ran while one was open for 5% of the time, Pallas kernels for 0%

commit v1 on v0

v1 whole, which is shorter than its diff:
```python
import functools

import jax
import jax.numpy as jnp
from jax import lax
from jax.experimental import pallas as pl
from jax.experimental.pallas import tpu as pltpu
from jax.sharding import PartitionSpec as P

SEQ = 128
EPSILON = 1e-06
MESH = pl.DeviceIdType.MESH
KINDS = (("in", True, False), ("out", False, False), ("up", True, True),
         ("down", False, True), ("gate", True, False))


def kernel(sizes, stream, in_w, out_w, up_w, down_w, gate_w, pool_w, scale,
           mix_gain, ffn_gain, result,
           in_all, out_all, up_all, down_all, gate_all,
           rows_all, normed, group_out, hidden, middle, mid_all,
           mix_send, mix_recv, ffn_send, ffn_recv,
           ring_send, ring_recv, fwd_send, fwd_recv, own_sem,
           tp_send, tp_recv, keep_sem):
    reps, fs, tp = sizes
    half = fs // 2
    my_rep, me, my_tp = lax.axis_index("rep"), lax.axis_index("fs"), lax.axis_index("tp")
    own = (in_w, out_w, up_w, down_w, gate_w)
    full = (in_all, out_all, up_all, down_all, gate_all)
    tokens, width = stream.shape

    def turn(at, by, count):
        return lax.rem(at + by + count, count)

    def piece(which, owner, row, count):
        block_rows, block_cols = own[which].shape
        if KINDS[which][1]:
            return full[which].at[pl.ds(pl.multiple_of(owner * block_rows + row, 16), count), :]
        return full[which].at[pl.ds(pl.multiple_of(row, 16), count),
                              pl.ds(pl.multiple_of(owner * block_cols, 128), block_cols)]

    def span(which, step, way):
        count = own[which].shape[0]
        row = 0
        if KINDS[which][2]:
            count = count // reps
            row = my_rep * count
        if step == half:
            count = count // 2
            row = row + way * count
        return row, count

    def ring(which, step, way):
        row, count = span(which, step, way)
        sign = 1 - 2 * way
        owner = turn(me, -sign * (step - 1), fs)
        if step == 1:
            source = own[which].at[pl.ds(pl.multiple_of(row, 16), count), :]
        else:
            source = piece(which, owner, row, count)
        return pltpu.make_async_remote_copy(
            src_ref=source, dst_ref=piece(which, owner, row, count),
            send_sem=ring_send.at[which, step - 1, way],
            recv_sem=ring_recv.at[which, step - 1, way],
            device_id={"fs": turn(me, sign, fs)}, device_id_type=MESH)

    def forward(which, step, way, peer):
        row, count = span(which, step, way)
        owner = turn(me, -(1 - 2 * way) * step, fs)
        block = piece(which, owner, row, count)
        shared = which - 2
        return pltpu.make_async_remote_copy(
            src_ref=block, dst_ref=block,
            send_sem=fwd_send.at[shared, peer - 1, step - 1, way],
            recv_sem=fwd_recv.at[shared, peer - 1, step - 1, way],
            device_id={"rep": turn(my_rep, peer, reps)}, device_id_type=MESH)

    def begin(which):
        for way in (0, 1):
            ring(which, 1, way).start()

    def advance(which, step):
        for way in (0, 1):
            ring(which, step, way).wait_recv()
            if step < half:
                ring(which, step + 1, way).start()
            if KINDS[which][2]:
                for peer in range(1, reps):
                    forward(which, step, way, peer).start()

    def tp_copy(stage, offset, source, target):
        return pltpu.make_async_remote_copy(
            src_ref=source, dst_ref=target,
            send_sem=tp_send.at[stage, offset - 1], recv_sem=tp_recv.at[stage, offset - 1],
            device_id={"tp": turn(my_tp, offset, tp)}, device_id_type=MESH)

    def feature_cols(owner):
        return pl.ds(pl.multiple_of(owner * width, 128), width)

    barrier = pltpu.get_barrier_semaphore()
    greeted = 0
    for name, at, count, offsets in (
            ("fs", me, fs, (1, -1)),
            ("tp", my_tp, tp, range(1, tp)),
            ("rep", my_rep, reps, range(1, reps))):
        for offset in offsets:
            pl.semaphore_signal(barrier, inc=1, device_id={name: turn(at, offset, count)},
                                device_id_type=MESH)
            greeted += 1
    pl.semaphore_wait(barrier, greeted)

    begin(0)
    begin(1)
    stream_sends = []
    for offset in range(1, tp):
        copy = tp_copy(0, offset, stream, rows_all.at[:, feature_cols(my_tp)])
        copy.start()
        stream_sends.append(copy)
    keeps = []
    for which in range(len(own)):
        keep = pltpu.make_async_copy(
            own[which], piece(which, me, 0, own[which].shape[0]), own_sem.at[which])
        keep.start()
        keeps.append(keep)
    keep_stream = pltpu.make_async_copy(
        stream, rows_all.at[:, feature_cols(my_tp)], keep_sem)
    keep_stream.start()
    for step in range(1, half):
        advance(0, step)
        advance(1, step)
    begin(2)
    begin(3)

    def norm_into(source, gain, target):
        tile = 64

        def body(i, carry):
            at = pl.ds(pl.multiple_of(i * tile, tile), tile)
            wide = source[at, :].astype(jnp.float32)
            mean = jnp.mean(wide * wide, axis=-1, keepdims=True)
            target[at, :] = (wide * lax.rsqrt(mean + EPSILON)
                             * gain[...].astype(jnp.float32)).astype(jnp.bfloat16)
            return carry

        lax.fori_loop(0, tokens // tile, body, 0)

    keep_stream.wait()
    for copy in stream_sends:
        copy.wait()
    norm_into(rows_all, mix_gain, normed)
    keeps[0].wait()
    advance(0, half)

    local_groups, group_dim = pool_w.shape[0], pool_w.shape[1]
    at_row = lax.broadcasted_iota(jnp.int32, (SEQ, SEQ), 0)
    at_col = lax.broadcasted_iota(jnp.int32, (SEQ, SEQ), 1)
    insides, inverses = [], []
    for g in range(local_groups):
        group = my_tp * local_groups + g
        level = lax.div(4 * group, local_groups * tp)
        reach = jnp.int32(2)
        for bit in range(1, 4):
            reach = jnp.where(level >= bit, jnp.int32(2 << bit), reach)
        inside = (at_col <= at_row) & (at_col > at_row - reach)
        insides.append(jnp.where(inside, 1.0, 0.0).astype(jnp.bfloat16))
        inverses.append(jnp.minimum(at_row + 1, reach).astype(jnp.float32)[:, :1])

    def mix(i, carry):
        at = pl.ds(pl.multiple_of(i * SEQ, SEQ), SEQ)
        pooled = jnp.dot(normed[at, :], in_all[...],
                         preferred_element_type=jnp.float32).astype(jnp.bfloat16)
        for g in range(local_groups):
            cols = slice(g * group_dim, (g + 1) * group_dim)
            part = pooled[:, cols]
            sums = jnp.dot(insides[g], part, preferred_element_type=jnp.float32)
            contrast = (sums / inverses[g] - part.astype(jnp.float32)).astype(jnp.bfloat16)
            mixed = jnp.dot(contrast, pool_w[g], preferred_element_type=jnp.float32)
            group_out[at, cols] = (mixed * scale[:, cols].astype(jnp.float32)).astype(jnp.bfloat16)
        return carry

    lax.fori_loop(0, tokens // SEQ, mix, 0)

    keeps[1].wait()
    advance(1, half)

    def spread(operand, weights, stage, sends, tile):
        def block(owner, target):
            def body(i, carry):
                at = pl.ds(pl.multiple_of(i * tile, tile), tile)
                target[at, :] = jnp.dot(operand[at, :], weights[:, feature_cols(owner)],
                                        preferred_element_type=jnp.float32).astype(jnp.bfloat16)
                return carry
            lax.fori_loop(0, tokens // tile, body, 0)

        copies = []
        recv = mix_recv if stage == 1 else ffn_recv
        for offset in sorted(range(1, tp), key=lambda o: -min(o, tp - o)):
            block(turn(my_tp, offset, tp), sends.at[offset - 1])
            copy = tp_copy(stage, offset, sends.at[offset - 1], recv.at[offset - 1])
            copy.start()
            copies.append(copy)
        block(my_tp, sends.at[tp - 1])
        return copies

    def gather_sum(base, recv, sends, target):
        tile = 64

        def body(i, carry):
            at = pl.ds(pl.multiple_of(i * tile, tile), tile)
            total = sends[tp - 1, at, :].astype(jnp.float32)
            for k in range(tp - 1):
                total = total + recv[k, at, :].astype(jnp.float32)
            target[at, :] = (base[at, :].astype(jnp.float32) + total).astype(jnp.bfloat16)
            return carry

        lax.fori_loop(0, tokens // tile, body, 0)

    mix_copies = spread(group_out, out_all, 1, mix_send, tokens // 2)
    for step in range(1, half):
        advance(2, step)
        advance(3, step)
    begin(4)
    for copy in mix_copies:
        copy.wait()
    gather_sum(stream, mix_recv, mix_send, middle)
    keep_middle = pltpu.make_async_copy(middle, mid_all.at[:, feature_cols(my_tp)], keep_sem)
    keep_middle.start()
    middle_copies = []
    for offset in range(1, tp):
        copy = tp_copy(2, offset, middle, mid_all.at[:, feature_cols(my_tp)])
        copy.start()
        middle_copies.append(copy)
    advance(2, half)
    advance(3, half)
    keep_middle.wait()
    for copy in middle_copies:
        copy.wait()
    norm_into(mid_all, ffn_gain, normed)
    for step in range(1, half + 1):
        advance(4, step)

    def arrived(which):
        keeps[which].wait()
        if KINDS[which][2]:
            for step in range(1, half + 1):
                for way in (0, 1):
                    for peer in range(1, reps):
                        forward(which, step, way, peer).wait()

    arrived(4)
    arrived(2)
    tile = tokens // 2

    def gated(i, carry):
        at = pl.ds(pl.multiple_of(i * tile, tile), tile)
        values = normed[at, :]
        gate = jnp.dot(values, gate_all[...], preferred_element_type=jnp.float32)
        up = jnp.dot(values, up_all[...], preferred_element_type=jnp.float32)
        hidden[at, :] = (gate / (1.0 + jnp.exp(-gate)) * up).astype(jnp.bfloat16)
        return carry

    lax.fori_loop(0, tokens // tile, gated, 0)
    arrived(3)
    ffn_copies = spread(hidden, down_all, 3, ffn_send, tokens // 2)
    for which in range(len(own)):
        for step in range(1, half + 1):
            for way in (0, 1):
                ring(which, step, way).wait_send()
    for copy in ffn_copies:
        copy.wait()
    gather_sum(middle, ffn_recv, ffn_send, result)


def on_device(sizes, stream, in_weight, pool_weight, pool_scale, out_weight,
              mix_gain, ffn_gain, gate_weight, up_weight, down_weight):
    reps, fs, tp = sizes
    half = fs // 2
    tokens, width = stream.shape
    features = width * tp
    own = (in_weight, out_weight, up_weight, down_weight, gate_weight)
    full = [pltpu.VMEM((w.shape[0] * fs, w.shape[1]) if kind[1] else (w.shape[0], w.shape[1] * fs),
                       jnp.bfloat16) for w, kind in zip(own, KINDS)]
    units = gate_weight.shape[1]
    bf = jnp.bfloat16
    vmem = pl.BlockSpec(memory_space=pltpu.VMEM)
    hbm = pl.BlockSpec(memory_space=pl.ANY)
    dma = pltpu.SemaphoreType.DMA
    flops = 2 * tokens * (2 * features * in_weight.shape[1] + 3 * features * units)
    return pl.pallas_call(
        functools.partial(kernel, sizes),
        out_shape=jax.ShapeDtypeStruct(stream.shape, bf),
        in_specs=[vmem] + [hbm] * 5 + [vmem] * 4,
        out_specs=vmem,
        scratch_shapes=full + [
            pltpu.VMEM((tokens, features), bf),
            pltpu.VMEM((tokens, features), bf),
            pltpu.VMEM((tokens, in_weight.shape[1]), bf),
            pltpu.VMEM((tokens, units), bf),
            pltpu.VMEM((tokens, width), bf),
            pltpu.VMEM((tokens, features), bf),
            pltpu.VMEM((tp, tokens, width), bf),
            pltpu.VMEM((tp - 1, tokens, width), bf),
            pltpu.VMEM((tp, tokens, width), bf),
            pltpu.VMEM((tp - 1, tokens, width), bf),
            dma((len(own), half, 2)),
            dma((len(own), half, 2)),
            dma((2, max(reps - 1, 1), half, 2)),
            dma((2, max(reps - 1, 1), half, 2)),
            dma((len(own),)),
            dma((4, tp - 1)),
            dma((4, tp - 1)),
            dma(()),
        ],
        compiler_params=pltpu.CompilerParams(
            collective_id=0, has_side_effects=True, vmem_limit_bytes=64 * 1024 * 1024 - 65536),
        cost_estimate=pl.CostEstimate(flops=flops, bytes_accessed=flops // 512, transcendentals=0),
    )(stream, in_weight, out_weight, up_weight, down_weight, gate_weight, pool_weight,
      pool_scale.reshape(1, -1), mix_gain.reshape(1, -1), ffn_gain.reshape(1, -1))


def solution(mesh):
    sizes = tuple(mesh.shape[name] for name in ("rep", "fs", "tp"))
    return jax.shard_map(
        functools.partial(on_device, sizes),
        mesh=mesh,
        in_specs=(
            P(("rep", "fs"), "tp"),
            P("fs", "tp"),
            P("tp", None, None),
            P("tp"),
            P("tp", "fs"),
            P(),
            P(),
            P("fs", "tp"),
            P("fs", "tp"),
            P("tp", "fs"),
        ),
        out_specs=P(("rep", "fs"), "tp"),
        check_vma=False,
    )
```

time: 516 us -> 266 us (0.52)
  waiting for transfers between devices: 457 us -> 0 us
  Pallas kernels: 0 us -> 260 us
  matrix products: 25.5 us -> 0 us
  between operations: 13.3 us -> 0.01 us
  other arithmetic: 9.67 us -> 0 us
    all_gather x8 -> x0, waiting for transfers between devices: 423 us -> none  [the longest x1 107 us: on_device(): lax.all_gather(down_weight, 'fs', axis=1, tiled=True)]
    pallas_call x0 -> x1, Pallas kernels: none -> 260 us  [on_device(): pl.pallas_call(functools.partial(kernel, sizes), out_shape=jax.ShapeDtype...]
    reduce_scatter x1 -> x0, waiting for transfers between devices: 29.6 us -> none  [on_device(): lax.psum_scatter(ffn_partials.astype(jnp.bfloat16), 'tp', scatter_dimensi...]
    dot_general x5 -> x0, matrix products: 25.5 us -> none  [the longest x1 13.4 us: on_device(): jnp.dot(hidden, down_rows, preferred_element_type=jnp.float32)]
  transfers between devices with their start and end apart: 10 -> 0, of which waited for: 10 -> 0; matrix products, arithmetic and copies ran while one was open for 5% -> 0% of each run, Pallas kernels for 0% -> 0%
where the time goes in v1:
time: 266 us
  Pallas kernels  260 us (98%)
  local copies, waits for them, and re-layouts  5.64 us (2%)
    pallas_call x1, Pallas kernels, on_device(): pl.pallas_call(functools.partial(kernel, sizes), out_shape=jax.ShapeDtype...  260 us

profile of v1, /device:TPU:0, one launch (start us, length us, event | category | flops | bytes accessed | tf_op | source)
XLA Modules:
  0.0 265.7 jit_solution(3659407756108465285)
XLA Ops:
  0.0 1.2 reshape.9.scale
  1.2 1.3 reshape.10.mix_gain
  2.5 1.3 reshape.11.ffn_gain
  3.8 260.1 %shard_map.100 = bf16[512,512]{1,0:T(8,128)(2,1)} custom-call(bf16[512,512]{1,0:T(8,128)(2,1)} %stream.1, bf16[512,256]{1,0:T(8,128)(2,1)} %in_w.1, bf16[256,512]{1,0:T(8,128)(2,1)} %out_w.1, bf16[512,1408]{1,0:T(8,128)(2,1)} %up_w.1, bf16[1408,512]{1,0:T(8,128)(2,1)} %down_w.1, bf16[512,1408]{1,0:T(8,128)(2,1)} %gate_w.1, bf16[2,128,128]{2,1,0:T(8,128)(2,1)} %pool_w.1, ...), custom_call_target="tpu_custom_call" | custom-call | flops 9932111872 | bytes 19398656 | tf_op jit(solution)/shard_map/pallas_call | solution.py:288
  263.9 1.9 copy.12

commit v2 on v1

--- a/solution.py
+++ b/solution.py
@@ -10,13 +10,14 @@
 SEQ = 128
 EPSILON = 1e-06
 MESH = pl.DeviceIdType.MESH
-KINDS = (("in", True, False), ("out", False, False), ("up", True, True),
-         ("down", False, True), ("gate", True, False))
-
-
-def kernel(sizes, stream, in_w, out_w, up_w, down_w, gate_w, pool_w, scale,
+BY_ROWS = (True, False, True, True, False)
+PIECES = ((0, 0), (1, 0), (2, 0), (3, 0), (2, 1), (3, 1), (4, 0), (4, 1))
+CHUNKS = (1, 1, 2, 2, 2)
+
+
+def kernel(sizes, stream, in_w, out_w, up_w, gate_w, down_w, pool_w, scale,
            mix_gain, ffn_gain, result,
-           in_all, out_all, up_all, down_all, gate_all,
+           in_all, out_all, up_all, gate_all, down_all,
            rows_all, normed, group_out, hidden, middle, mid_all,
            mix_send, mix_recv, ffn_send, ffn_recv,
            ring_send, ring_recv, fwd_send, fwd_recv, own_sem,
@@ -24,8 +25,8 @@
     reps, fs, tp = sizes
     half = fs // 2
     my_rep, me, my_tp = lax.axis_index("rep"), lax.axis_index("fs"), lax.axis_index("tp")
-    own = (in_w, out_w, up_w, down_w, gate_w)
-    full = (in_all, out_all, up_all, down_all, gate_all)
+    own = (in_w, out_w, up_w, gate_w, down_w)
+    full = (in_all, out_all, up_all, gate_all, down_all)
     tokens, width = stream.shape
 
     def turn(at, by, count):
@@ -33,24 +34,29 @@
 
     def piece(which, owner, row, count):
         block_rows, block_cols = own[which].shape
-        if KINDS[which][1]:
+        if BY_ROWS[which]:
             return full[which].at[pl.ds(pl.multiple_of(owner * block_rows + row, 16), count), :]
         return full[which].at[pl.ds(pl.multiple_of(row, 16), count),
                               pl.ds(pl.multiple_of(owner * block_cols, 128), block_cols)]
 
-    def span(which, step, way):
-        count = own[which].shape[0]
-        row = 0
-        if KINDS[which][2]:
-            count = count // reps
-            row = my_rep * count
+    def span(number, step, way):
+        which, chunk = PIECES[number]
+        rows = own[which].shape[0]
+        cut = rows % (CHUNKS[which] * reps * 2 * 16) == 0
+        count = rows // CHUNKS[which] if cut else (rows, 0)[chunk]
+        row = chunk * (rows // CHUNKS[which])
+        count = count // reps
+        row = row + my_rep * count
         if step == half:
             count = count // 2
             row = row + way * count
-        return row, count
-
-    def ring(which, step, way):
-        row, count = span(which, step, way)
+        return which, row, count
+
+    def empty(number):
+        return span(number, 1, 0)[2] == 0
+
+    def ring(number, step, way):
+        which, row, count = span(number, step, way)
         sign = 1 - 2 * way
         owner = turn(me, -sign * (step - 1), fs)
         if step == 1:
@@ -59,33 +65,54 @@
             source = piece(which, owner, row, count)
         return pltpu.make_async_remote_copy(
             src_ref=source, dst_ref=piece(which, owner, row, count),
-            send_sem=ring_send.at[which, step - 1, way],
-            recv_sem=ring_recv.at[which, step - 1, way],
+            send_sem=ring_send.at[number, step - 1, way],
+            recv_sem=ring_recv.at[number, step - 1, way],
             device_id={"fs": turn(me, sign, fs)}, device_id_type=MESH)
 
-    def forward(which, step, way, peer):
-        row, count = span(which, step, way)
-        owner = turn(me, -(1 - 2 * way) * step, fs)
-        block = piece(which, owner, row, count)
-        shared = which - 2
+    def forward(number, step, way, peer):
+        which, row, count = span(number, step, way)
+        block = piece(which, turn(me, -(1 - 2 * way) * step, fs), row, count)
         return pltpu.make_async_remote_copy(
             src_ref=block, dst_ref=block,
-            send_sem=fwd_send.at[shared, peer - 1, step - 1, way],
-            recv_sem=fwd_recv.at[shared, peer - 1, step - 1, way],
+            send_sem=fwd_send.at[number, peer - 1, step - 1, way],
+            recv_sem=fwd_recv.at[number, peer - 1, step - 1, way],
             device_id={"rep": turn(my_rep, peer, reps)}, device_id_type=MESH)
 
-    def begin(which):
+    def begin(*numbers):
+        for number in numbers:
+            if not empty(number):
+                for way in (0, 1):
+                    ring(number, 1, way).start()
+
+    def advance(number, step):
+        if empty(number):
+            return
         for way in (0, 1):
-            ring(which, 1, way).start()
-
-    def advance(which, step):
-        for way in (0, 1):
-            ring(which, step, way).wait_recv()
+            ring(number, step, way).wait_recv()
             if step < half:
-                ring(which, step + 1, way).start()
-            if KINDS[which][2]:
-                for peer in range(1, reps):
-                    forward(which, step, way, peer).start()
+                ring(number, step + 1, way).start()
+            for peer in range(1, reps):
+                forward(number, step, way, peer).start()
+
+    def early(*numbers):
+        for number in numbers:
+            for step in range(1, half):
+                advance(number, step)
+
+    def late(*numbers):
+        for number in numbers:
+            advance(number, half)
+
+    def arrived(*numbers):
+        for number in numbers:
+            if PIECES[number][1] == 0:
+                keeps[PIECES[number][0]].wait()
+            if empty(number):
+                continue
+            for step in range(1, half + 1):
+                for way in (0, 1):
+                    for peer in range(1, reps):
+                        forward(number, step, way, peer).wait()
 
     def tp_copy(stage, offset, source, target):
         return pltpu.make_async_remote_copy(
@@ -108,8 +135,7 @@
             greeted += 1
     pl.semaphore_wait(barrier, greeted)
 
-    begin(0)
-    begin(1)
+    begin(0, 1)
     stream_sends = []
     for offset in range(1, tp):
         copy = tp_copy(0, offset, stream, rows_all.at[:, feature_cols(my_tp)])
@@ -124,11 +150,9 @@
     keep_stream = pltpu.make_async_copy(
         stream, rows_all.at[:, feature_cols(my_tp)], keep_sem)
     keep_stream.start()
-    for step in range(1, half):
-        advance(0, step)
-        advance(1, step)
-    begin(2)
-    begin(3)
+    early(0, 1)
+    begin(2, 3, 4)
+    late(0, 1)
 
     def norm_into(source, gain, target):
         tile = 64
@@ -147,8 +171,7 @@
     for copy in stream_sends:
         copy.wait()
     norm_into(rows_all, mix_gain, normed)
-    keeps[0].wait()
-    advance(0, half)
+    arrived(0)
 
     local_groups, group_dim = pool_w.shape[0], pool_w.shape[1]
     at_row = lax.broadcasted_iota(jnp.int32, (SEQ, SEQ), 0)
@@ -179,8 +202,8 @@
 
     lax.fori_loop(0, tokens // SEQ, mix, 0)
 
-    keeps[1].wait()
-    advance(1, half)
+    arrived(1)
+    early(2)
 
     def spread(operand, weights, stage, sends, tile):
         def block(owner, target):
@@ -215,10 +238,8 @@
         lax.fori_loop(0, tokens // tile, body, 0)
 
     mix_copies = spread(group_out, out_all, 1, mix_send, tokens // 2)
-    for step in range(1, half):
-        advance(2, step)
-        advance(3, step)
-    begin(4)
+    early(3)
+    begin(5)
     for copy in mix_copies:
         copy.wait()
     gather_sum(stream, mix_recv, mix_send, middle)
@@ -229,25 +250,20 @@
         copy = tp_copy(2, offset, middle, mid_all.at[:, feature_cols(my_tp)])
         copy.start()
         middle_copies.append(copy)
-    advance(2, half)
-    advance(3, half)
+    early(4)
+    begin(6, 7)
+    late(2, 3)
     keep_middle.wait()
     for copy in middle_copies:
         copy.wait()
     norm_into(mid_all, ffn_gain, normed)
-    for step in range(1, half + 1):
-        advance(4, step)
-
-    def arrived(which):
-        keeps[which].wait()
-        if KINDS[which][2]:
-            for step in range(1, half + 1):
-                for way in (0, 1):
-                    for peer in range(1, reps):
-                        forward(which, step, way, peer).wait()
-
-    arrived(4)
-    arrived(2)
+    early(5)
+    late(4)
+    early(6)
+    late(5)
+    early(7)
+    late(6)
+    arrived(2, 3, 4, 5)
     tile = tokens // 2
 
     def gated(i, carry):
@@ -259,12 +275,14 @@
         return carry
 
     lax.fori_loop(0, tokens // tile, gated, 0)
-    arrived(3)
+    late(7)
+    arrived(6, 7)
     ffn_copies = spread(hidden, down_all, 3, ffn_send, tokens // 2)
-    for which in range(len(own)):
-        for step in range(1, half + 1):
-            for way in (0, 1):
-                ring(which, step, way).wait_send()
+    for number in range(len(PIECES)):
+        if not empty(number):
+            for step in range(1, half + 1):
+                for way in (0, 1):
+                    ring(number, step, way).wait_send()
     for copy in ffn_copies:
         copy.wait()
     gather_sum(middle, ffn_recv, ffn_send, result)
@@ -276,9 +294,9 @@
     half = fs // 2
     tokens, width = stream.shape
     features = width * tp
-    own = (in_weight, out_weight, up_weight, down_weight, gate_weight)
-    full = [pltpu.VMEM((w.shape[0] * fs, w.shape[1]) if kind[1] else (w.shape[0], w.shape[1] * fs),
-                       jnp.bfloat16) for w, kind in zip(own, KINDS)]
+    own = (in_weight, out_weight, up_weight, gate_weight, down_weight)
+    full = [pltpu.VMEM((w.shape[0] * fs, w.shape[1]) if by_rows else (w.shape[0], w.shape[1] * fs),
+                       jnp.bfloat16) for w, by_rows in zip(own, BY_ROWS)]
     units = gate_weight.shape[1]
     bf = jnp.bfloat16
     vmem = pl.BlockSpec(memory_space=pltpu.VMEM)
@@ -301,10 +319,10 @@
             pltpu.VMEM((tp - 1, tokens, width), bf),
             pltpu.VMEM((tp, tokens, width), bf),
             pltpu.VMEM((tp - 1, tokens, width), bf),
-            dma((len(own), half, 2)),
-            dma((len(own), half, 2)),
-            dma((2, max(reps - 1, 1), half, 2)),
-            dma((2, max(reps - 1, 1), half, 2)),
+            dma((len(PIECES), half, 2)),
+            dma((len(PIECES), half, 2)),
+            dma((len(PIECES), max(reps - 1, 1), half, 2)),
+            dma((len(PIECES), max(reps - 1, 1), half, 2)),
             dma((len(own),)),
             dma((4, tp - 1)),
             dma((4, tp - 1)),
@@ -313,7 +331,7 @@
         compiler_params=pltpu.CompilerParams(
             collective_id=0, has_side_effects=True, vmem_limit_bytes=64 * 1024 * 1024 - 65536),
         cost_estimate=pl.CostEstimate(flops=flops, bytes_accessed=flops // 512, transcendentals=0),
-    )(stream, in_weight, out_weight, up_weight, down_weight, gate_weight, pool_weight,
+    )(stream, in_weight, out_weight, up_weight, gate_weight, down_weight, pool_weight,
       pool_scale.reshape(1, -1), mix_gain.reshape(1, -1), ffn_gain.reshape(1, -1))
 
 

time: 266 us -> 217 us (0.82)
  Pallas kernels: 260 us -> 211 us
    pallas_call x1, Pallas kernels: 260 us -> 211 us  [on_device(): pl.pallas_call(functools.partial(kernel, sizes), out_shape=jax.ShapeDtype...]
where the time goes in v2:
time: 217 us
  Pallas kernels  211 us (97%)
  local copies, waits for them, and re-layouts  5.64 us (3%)
    pallas_call x1, Pallas kernels, on_device(): pl.pallas_call(functools.partial(kernel, sizes), out_shape=jax.ShapeDtype...  211 us

profile of v2, /device:TPU:0, one launch (start us, length us, event | category | flops | bytes accessed | tf_op | source)
XLA Modules:
  0.0 217.1 jit_solution(5617818154700964250)
XLA Ops:
  0.0 1.2 reshape.9.scale
  1.2 1.3 reshape.10.mix_gain
  2.5 1.3 reshape.11.ffn_gain
  3.8 211.4 %shard_map.100 = bf16[512,512]{1,0:T(8,128)(2,1)} custom-call(bf16[512,512]{1,0:T(8,128)(2,1)} %stream.1, bf16[512,256]{1,0:T(8,128)(2,1)} %in_w.1, bf16[256,512]{1,0:T(8,128)(2,1)} %out_w.1, bf16[512,1408]{1,0:T(8,128)(2,1)} %up_w.1, bf16[512,1408]{1,0:T(8,128)(2,1)} %gate_w.1, bf16[1408,512]{1,0:T(8,128)(2,1)} %down_w.1, bf16[2,128,128]{2,1,0:T(8,128)(2,1)} %pool_w.1, ...), custom_call_target="tpu_custom_call" | custom-call | flops 9932111872 | bytes 19398656 | tf_op jit(solution)/shard_map/pallas_call | solution.py:306
  215.2 1.9 copy.12
